TPU v7x, 32 devices: a whole 2x2x4 slice. The times are simulated.
32 devices in a mesh: sp: 8 (over z, y), tp: 4 (over x, core).
Axes of the slice: x: 2, y: 2, z: 4, core: 2. Of those that a mesh axis runs over, the one named last changes fastest.
Arguments:
- latents: bfloat16 [2560, 2048], P(('sp', 'tp')), may hold values from -12.5 to 12.5, as said below
- context: bfloat16 [1024, 2048], P('sp'), may hold values from -120 to 120, as said below
- cond_vec: float32 [2048], replicated, may hold values from -6 to 6
- ctx_vec: float32 [2048], replicated, may hold values from -6 to 6
- shift_w: bfloat16 [2048, 2048], P('sp', 'tp'), may hold values from -0.125 to 0.125
- scale_w: bfloat16 [2048, 2048], P('sp', 'tp'), may hold values from -0.125 to 0.125
- modgate_w: bfloat16 [2048, 2048], P('sp', 'tp'), may hold values from -0.125 to 0.125
- query_down_weight: bfloat16 [2048, 512], replicated, may hold values from -0.125 to 0.125
- latent_down_weight: bfloat16 [2048, 256], replicated, may hold values from -0.125 to 0.125
- rot_down: bfloat16 [2048, 32], replicated, may hold values from -0.125 to 0.125
- gate_w: bfloat16 [2048, 2048], P(None, 'tp'), may hold values from -0.125 to 0.125
- query_norm_gain: float32 [512], replicated, may hold values from 0.1 to 1.9
- latent_norm_gain: float32 [256], replicated, may hold values from 0.1 to 1.9
- query_plain_weight: bfloat16 [512, 2048], P(None, 'tp'), may hold values from -0.25 to 0.25
- query_rotary_weight: bfloat16 [512, 1024], P(None, 'tp'), may hold values from -0.25 to 0.25
- key_expand_weight: bfloat16 [256, 2048], P(None, 'tp'), may hold values from -0.375 to 0.375
- value_expand_weight: bfloat16 [256, 2048], P(None, 'tp'), may hold values from -0.375 to 0.375
- out_w: bfloat16 [2048, 2048], P('tp'), may hold values from -0.5 to 0.5
- norm_gain: float32 [2048], replicated, may hold values from 0.1 to 1.9
- norm_bias: float32 [2048], replicated, may hold values from -3 to 3
Outputs:
- mixed_out: bfloat16 [2560, 2048], P(('sp', 'tp'))
Inputs may be any that keep to these rules, and one draw needn't show every extreme that they name: `latents`: latent rows are noise plus three slow waves along the whole sequence. Most context rows have their own scales of 1 to 3; a few rows may be far larger.
All inputs are finite; a program needn't handle non-finite values.
Results may differ from a plain program's by a relative error of at most 0.024.
The roundings to bfloat16 on the way count: a program that leaves them out, or rounds other values in their place, can miss the bound.
Values may be sent and summed in bfloat16 or wider, within the bound.
No kernel may reach another device: no remote copies, remote signals or barrier semaphores. Data moves between devices by JAX's collectives and lax.ppermute only.
A program may use at most 128 MiB of HBM per device.

v0:
```python
import jax
import jax.numpy as jnp
from jax import lax
from jax.sharding import PartitionSpec as P

PLAIN_HEAD_SIZE = 64
ROTARY_SIZE = 32
VALUE_HEAD_SIZE = 64
GRID_W = 64
rope_base = 10000.0
norm_floor = 1e-06
residual_weight = 2.0**0.5
score_floor = -1e30


def rms_scale(values, gain):
    return values * lax.rsqrt(jnp.mean(values * values, axis=-1, keepdims=True) + norm_floor) * gain


def rotate(values, positions):
    pair_count = ROTARY_SIZE // 4
    inverse = rope_base ** (-jnp.arange(pair_count, dtype=jnp.float32) / pair_count)
    grid_row = (positions // GRID_W).astype(jnp.float32)
    grid_col = (positions % GRID_W).astype(jnp.float32)
    angles = jnp.stack([grid_row[:, None] * inverse, grid_col[:, None] * inverse], axis=1)
    cosine = jnp.cos(angles)[:, None, :, None, :]
    sine_part = jnp.sin(angles)[:, None, :, None, :]
    shaped = values.reshape(values.shape[0], -1, 2, 2, pair_count)
    first_part = shaped[:, :, :, 0:1, :]
    second = shaped[:, :, :, 1:2, :]
    turned = jnp.concatenate(
        [first_part * cosine - second * sine_part, second * cosine + first_part * sine_part], axis=3
    )
    return turned.reshape(values.shape)


def project(rows, weight):
    return jnp.dot(rows, weight, preferred_element_type=jnp.float32)


def per_device(
    latents,
    context,
    cond_vec,
    ctx_vec,
    shift_w,
    scale_w,
    modgate_w,
    query_down_weight,
    latent_down_weight,
    rot_down,
    gate_w,
    query_norm_gain,
    latent_norm_gain,
    query_plain_weight,
    query_rotary_weight,
    key_expand_weight,
    value_expand_weight,
    out_w,
    norm_gain,
    norm_bias,
):
    width_tp = lax.axis_size("tp")
    block_rows = latents.shape[0]
    seq_rows = block_rows * width_tp
    slab_rows = shift_w.shape[0]
    sp_index = lax.axis_index("sp")
    cond_rows = jnp.stack([jax.nn.silu(cond_vec), jax.nn.silu(ctx_vec)]).astype(jnp.bfloat16)
    cond_here = lax.dynamic_slice_in_dim(cond_rows, sp_index * slab_rows, slab_rows, 1)
    shift_part = project(cond_here, shift_w)
    scale_part = project(cond_here, scale_w)
    gate_part = project(cond_here, modgate_w)
    columns = shift_w.shape[1]
    corner = (jnp.int32(0), lax.axis_index("tp") * columns)
    blank_rows = jnp.zeros((2, latents.shape[1]), jnp.float32)
    shift_vec, scale_vec, gate_vec = lax.psum(
        (
            lax.dynamic_update_slice(blank_rows, shift_part, corner),
            lax.dynamic_update_slice(blank_rows, scale_part, corner),
            lax.dynamic_update_slice(blank_rows, gate_part, corner),
        ),
        ("sp", "tp"),
    )
    latent_in = (latents.astype(jnp.float32) * (1.0 + scale_vec[0]) + shift_vec[0]).astype(
        jnp.bfloat16
    )
    context_in = (context.astype(jnp.float32) * (1.0 + scale_vec[1]) + shift_vec[1]).astype(
        jnp.bfloat16
    )
    heads_here = gate_w.shape[1] // VALUE_HEAD_SIZE
    rows_part = lax.all_gather(latent_in, "tp", axis=0, tiled=True)
    positions = sp_index * seq_rows + jnp.arange(rows_part.shape[0], dtype=jnp.int32)
    q_codes = rms_scale(project(rows_part, query_down_weight), query_norm_gain).astype(jnp.bfloat16)
    kv_codes = rms_scale(project(rows_part, latent_down_weight), latent_norm_gain).astype(
        jnp.bfloat16
    )
    key_rot = rotate(project(rows_part, rot_down), positions).astype(jnp.bfloat16)
    gate_act = project(rows_part, gate_w).astype(jnp.bfloat16)
    project_q_cont = project(q_codes, query_plain_weight).astype(jnp.bfloat16)
    project_q_rot = rotate(project(q_codes, query_rotary_weight), positions).astype(jnp.bfloat16)
    joined = jnp.concatenate([project_q_cont, project_q_rot, gate_act, kv_codes, key_rot], axis=1)
    edge_one = query_plain_weight.shape[1]
    edge_two = edge_one + query_rotary_weight.shape[1]
    edge_three = edge_two + gate_w.shape[1]
    edge_four = edge_three + latent_down_weight.shape[1]
    q_cont = joined[:, :edge_one].reshape(seq_rows, heads_here, PLAIN_HEAD_SIZE)
    q_rot = joined[:, edge_one:edge_two].reshape(seq_rows, heads_here, ROTARY_SIZE)
    gate_act = joined[:, edge_two:edge_three]
    kv_codes = joined[:, edge_three:edge_four]
    key_rot = joined[:, edge_four:]
    ctx_codes = rms_scale(project(context_in, latent_down_weight), latent_norm_gain).astype(
        jnp.bfloat16
    )
    ctx_rot = project(context_in, rot_down).astype(jnp.bfloat16)
    score_scale = (PLAIN_HEAD_SIZE + ROTARY_SIZE) ** (-0.5)

    def expand(codes):
        return (
            project(codes, key_expand_weight).astype(jnp.bfloat16),
            project(codes, value_expand_weight).astype(jnp.bfloat16),
        )

    def attend(running, key_block, value_block, rotary):
        row_top, row_total, weighted = running
        key_count = key_block.shape[0]
        scores = jnp.einsum(
            "qhd,khd->hqk",
            q_cont,
            key_block.reshape(key_count, heads_here, PLAIN_HEAD_SIZE),
            preferred_element_type=jnp.float32,
        )
        scores = (
            scores + jnp.einsum("qhd,kd->hqk", q_rot, rotary, preferred_element_type=jnp.float32)
        ) * score_scale
        new_top = jnp.maximum(row_top, jnp.max(scores, axis=-1))
        weights = jnp.exp(scores - new_top[:, :, None])
        factor = jnp.exp(row_top - new_top)
        row_total = row_total * factor + jnp.sum(weights, axis=-1)
        weighted = weighted * factor[:, :, None] + jnp.einsum(
            "hqk,khd->hqd",
            weights.astype(jnp.bfloat16),
            value_block.reshape(key_count, heads_here, VALUE_HEAD_SIZE),
            preferred_element_type=jnp.float32,
        )
        return (new_top, row_total, weighted)

    start_state = (
        jnp.full((heads_here, seq_rows), score_floor, jnp.float32),
        jnp.zeros((heads_here, seq_rows), jnp.float32),
        jnp.zeros((heads_here, seq_rows, VALUE_HEAD_SIZE), jnp.float32),
    )
    ctx_all_codes, ctx_all_rot = (
        lax.all_gather(ctx_codes, "sp", axis=0, tiled=True),
        lax.all_gather(ctx_rot, "sp", axis=0, tiled=True),
    )
    ctx_keys, ctx_values = expand(ctx_all_codes)
    running = attend(start_state, ctx_keys, ctx_values, ctx_all_rot)
    pieces = (
        lax.all_gather(kv_codes, "sp", axis=0, tiled=True),
        lax.all_gather(key_rot, "sp", axis=0, tiled=True),
    )
    total_rows = pieces[0].shape[0]
    unit_count = total_rows // seq_rows
    grouped = max(
        [1]
        + [
            divisor
            for divisor in range(1, unit_count + 1)
            if unit_count % divisor == 0 and divisor * seq_rows <= 1024
        ]
    )
    blocked = tuple(
        (
            member.reshape(unit_count // grouped, grouped * seq_rows, member.shape[1])
            for member in pieces
        )
    )

    def one_block(carried, members):
        key_block, value_block = expand(members[0])
        return (attend(carried, key_block, value_block, members[1]), None)

    result, unused = lax.scan(one_block, running, blocked)
    running = result
    row_top, row_total, weighted = running
    attended = jnp.transpose(weighted / row_total[:, :, None], (1, 0, 2)).reshape(
        seq_rows, heads_here * VALUE_HEAD_SIZE
    )
    gated = (attended * jax.nn.silu(gate_act.astype(jnp.float32))).astype(jnp.bfloat16)
    branch = lax.psum_scatter(
        project(gated, out_w).astype(jnp.bfloat16), "tp", scatter_dimension=0, tiled=True
    ).astype(jnp.float32)
    blended = residual_weight * latents.astype(jnp.float32) + gate_vec[0] * branch
    row_mean = jnp.mean(blended, axis=-1, keepdims=True)
    centred = blended - row_mean
    row_var = jnp.mean(centred * centred, axis=-1, keepdims=True)
    return (centred * lax.rsqrt(row_var + norm_floor) * norm_gain + norm_bias).astype(jnp.bfloat16)


def solution(mesh):
    in_specs = (
        P(("sp", "tp"), None),
        P("sp", None),
        P(),
        P(),
        P("sp", "tp"),
        P("sp", "tp"),
        P("sp", "tp"),
        P(),
        P(),
        P(),
        P(None, "tp"),
        P(),
        P(),
        P(None, "tp"),
        P(None, "tp"),
        P(None, "tp"),
        P(None, "tp"),
        P("tp", None),
        P(),
        P(),
    )
    out_specs = P(("sp", "tp"), None)
    return jax.shard_map(
        per_device, mesh=mesh, in_specs=in_specs, out_specs=out_specs, check_vma=False
    )
```

profile of v0, /device:TPU:0, one launch (start us, length us, event | category | flops | bytes accessed | tf_op | source)
XLA Modules:
  0.0 249.4 jit_solution(9773118889546091030)
XLA Ops:
  11.7 42.5 %all-reduce = (f32[2,2048]{1,0:T(2,128)S(1)}, f32[2,2048]{1,0:T(2,128)S(1)}, f32[2,2048]{1,0:T(2,128)S(1)}) all-reduce(f32[2,2048]{1,0:T(2,128)S(1)} %convolution_dynamic-update-slice_fusion, f32[2,2048]{1,0:T(2,128)S(1)} %convolution_dynamic-update-slice_fusion.1, ...), channel_id=1, replica_groups=mesh['sp'=8,'tp'=4] {'sp','tp'}, use_global_device_ids=true, to_apply=%region_2.3 | all-reduce | flops 12288 | bytes 98304 | tf_op jit(solution)/shard_map/psum | solution.py:76
  54.2 1.8 fusion.30
  57.4 26.1 %all_gather.17 = bf16[1024,32]{0,1:T(8,128)(2,1)S(1)} all-gather(bf16[128,32]{0,1:T(8,128)(2,1)S(1)} %convolution_convert_fusion.7), channel_id=1, replica_groups=mesh['sp'=8,'tp'=4] {'sp'}, dimensions={0}, use_global_device_ids=true | all-gather | bytes 73728 | tf_op jit(solution)/shard_map/all_gather | solution.py:154
  83.7 1.6 multiply_reduce_fusion.3
  85.4 31.5 %all_gather.16 = bf16[1024,256]{1,0:T(8,128)(2,1)S(1)} all-gather(bf16[128,256]{1,0:T(8,128)(2,1)S(1)} %multiply_convert_fusion.3), channel_id=1, replica_groups=mesh['sp'=8,'tp'=4] {'sp'}, dimensions={0}, use_global_device_ids=true | all-gather | bytes 589824 | tf_op jit(solution)/shard_map/all_gather | solution.py:153
  119.9 3.0 %multiply_reduce_fusion.1 = (f32[320]{0:T(512)S(1)}, f32[320,512]{1,0:T(8,128)S(1)}) fusion(bf16[320,2048]{1,0:T(8,128)(2,1)} %all-gather.4.cloned.1.call-done, bf16[2048,512]{1,0:T(8,128)(2,1)} %param.29), kind=kOutput, calls=%fused_computation.49 | convolution fusion | flops 671416000 | bytes 4064512 | tf_op jit(solution)/shard_map/dot_general | solution.py:38
  123.9 2.2 multiply_reduce_fusion.2
  127.0 1.8 fusion.58
  129.0 31.2 %all-gather = bf16[8,320,32]{1,2,0:T(8,128)(2,1)S(1)} all-gather(bf16[1,320,32]{1,2,0:T(8,128)(2,1)S(1)} %bitcast.115), channel_id=1, replica_groups=mesh['sp'=8,'tp'=4] {'sp'}, dimensions={0}, use_global_device_ids=true | all-gather | bytes 184320 | tf_op jit(solution)/shard_map/all_gather | solution.py:160
  162.8 1.8 fusion.56
  164.6 2.1 fusion.20
  166.7 2.2 fusion.24
  169.0 37.6 %while.14 = (s32[]{:T(128)}, f32[8,320]{1,0:T(8,128)S(1)}, f32[8,320]{1,0:T(8,128)S(1)}, f32[8,320,64]{1,2,0:T(8,128)S(1)}, bf16[4,640,256]{2,1,0:T(8,128)(2,1)}...) while((s32[]{:T(128)}, f32[8,320]{1,0:T(8,128)S(1)}, ...), condition=%wide.region_11.12_spmd, body=%wide.region_8.11_spmd.sunk | while | flops 872289280 | bytes 39624860 | solution.py:183
  171.6 2.2 fusion.112
  176.7 1.7 fusion.114
  181.0 2.2 fusion.112
  186.1 1.7 fusion.114
  190.3 2.2 fusion.112
  195.5 1.7 fusion.114
  199.7 2.2 fusion.112
  204.9 1.7 fusion.114
  209.0 4.8 %convolution_convert_fusion.2 = bf16[320,2048]{1,0:T(8,128)(2,1)} fusion(bf16[512,2048]{1,0:T(8,128)(2,1)S(1)} %copy-done, f32[320,512]{1,0:T(8,128)S(1)} %copy.40, bf16[320,2048]{1,0:T(8,128)(2,1)} %all-gather.4.cloned.1.call-done, bf16[2048,512]{1,0:T(8,128)(2,1)} %param.32), kind=kOutput, calls=%fused_computation.28 | convolution fusion | flops 1344143360 | bytes 7471104 | tf_op jit(solution)/shard_map/dot_general | solution.py:38
  213.8 24.7 %reduce-scatter.2.cloned.1.call-done = bf16[80,2048]{1,0:T(8,128)(2,1)} async-done(((bf16[320,2048]{1,0:T(8,128)(2,1)}), bf16[80,2048]{1,0:T(8,128)(2,1)}) %reduce-scatter.2.cloned.1.call-update) | async-done | bytes 327696 | tf_op jit(solution)/shard_map/reduce_scatter | solution.py:190
  241.0 1.9 add_convert_fusion.1
  (115 shorter events, 41.1 us)
Async XLA Ops:
  6.5 202.4 %copy-start = (bf16[512,2048]{1,0:T(8,128)(2,1)S(1)}, bf16[512,2048]{1,0:T(8,128)(2,1)}, u32[]{:S(2)}) copy-start(bf16[512,2048]{1,0:T(8,128)(2,1)} %param.39) | copy-start | bytes 6291460
  6.5 77.2 %copy-start.14 = (bf16[128,2048]{1,0:T(8,128)(2,1)S(1)}, bf16[128,2048]{1,0:T(8,128)(2,1)}, u32[]{:S(2)}) copy-start(bf16[128,2048]{1,0:T(8,128)(2,1)} %param.23) | copy-start | bytes 1572868
  6.5 78.8 %copy-start.13 = (f32[256]{0:T(256)S(1)}, f32[256]{0:T(256)}, u32[]{:S(2)}) copy-start(f32[256]{0:T(256)} %param.34) | copy-start | bytes 3076
  6.5 113.3 %all-gather.4.cloned.1.call-start = ((), (), s32[]{:S(2)}) async-start(), calls=%async_computation.1 | async-start | bytes 1638400 | tf_op jit(solution)/shard_map/all_gather | solution.py:91
  10.5 106.4 %copy-start.1 = (bf16[256,512]{1,0:T(8,128)(2,1)S(1)}, bf16[256,512]{1,0:T(8,128)(2,1)}, u32[]{:S(2)}) copy-start(bf16[256,512]{1,0:T(8,128)(2,1)} %param.37) | copy-start | bytes 786436
  56.0 113.0 %all-gather.6.cloned.1.call-start = ((), (), s32[]{:S(2)}) async-start(), calls=%async_computation.2 | async-start | bytes 1474560 | tf_op jit(solution)/shard_map/all_gather | solution.py:159
  56.1 62.3 %copy-start.2 = (bf16[256,512]{1,0:T(8,128)(2,1)S(1)}, bf16[256,512]{1,0:T(8,128)(2,1)}, u32[]{:S(2)}) copy-start(bf16[256,512]{1,0:T(8,128)(2,1)} %param.38) | copy-start | bytes 786436
  119.9 3.0 %copy-start.8 = (bf16[512,256]{1,0:T(8,128)(2,1)S(1)}, bf16[512,256]{1,0:T(8,128)(2,1)}, u32[]{:S(2)}) copy-start(bf16[512,256]{1,0:T(8,128)(2,1)} %param.36) | copy-start | bytes 786436
  119.9 3.0 %copy-start.12 = (f32[512]{0:T(512)S(1)}, f32[512]{0:T(512)}, u32[]{:S(2)}) copy-start(f32[512]{0:T(512)} %param.33) | copy-start | bytes 6148
  119.9 3.4 %copy-start.7 = (bf16[512,512]{1,0:T(8,128)(2,1)S(1)}, bf16[512,512]{1,0:T(8,128)(2,1)}, u32[]{:S(2)}) copy-start(bf16[512,512]{1,0:T(8,128)(2,1)} %param.35) | copy-start | bytes 1572868
  123.7 3.3 %copy-start.9 = (bf16[2048,32]{0,1:T(8,128)(2,1)S(1)}, bf16[2048,32]{0,1:T(8,128)(2,1)}, u32[]{:S(2)}) copy-start(bf16[2048,32]{0,1:T(8,128)(2,1)} %param.31) | copy-start | bytes 393220
  127.0 111.5 %reduce-scatter.2.cloned.1.call-start = ((), (), s32[]{:S(2)}) async-start(), calls=%async_computation.3 | async-start | bytes 1638400 | tf_op jit(solution)/shard_map/reduce_scatter | solution.py:190
  161.2 1.6 copy-start.5
  164.6 2.2 copy-start.6
  173.7 1.6 copy-start.3
  183.1 1.6 copy-start.3
  192.5 1.6 copy-start.3
  201.9 1.6 copy-start.3
  209.0 29.5 %copy-start.4 = (bf16[80,2048]{1,0:T(8,128)(2,1)S(1)}, bf16[80,2048]{1,0:T(8,128)(2,1)}, u32[]{:S(2)}) copy-start(bf16[80,2048]{1,0:T(8,128)(2,1)} %param.22) | copy-start | bytes 983044
  213.8 27.2 %copy-start.10 = (f32[2048]{0:T(1024)S(1)}, f32[2048]{0:T(1024)}, u32[]{:S(2)}) copy-start(f32[2048]{0:T(1024)} %param.41) | copy-start | bytes 24580
  213.8 27.2 %copy-start.11 = (f32[2048]{0:T(1024)S(1)}, f32[2048]{0:T(1024)}, u32[]{:S(2)}) copy-start(f32[2048]{0:T(1024)} %param.40) | copy-start | bytes 24580
Sparse Core Ops, SparseCore 0:
  56.1 17.9 all-gather.3
  127.1 40.2 all-gather.5
  213.9 24.5 reduce-scatter.1
where the time goes:
time: 251 us; the launch traced here: 249 us
  blocking collectives  131 us (52%)
  matrix products  58.6 us (23%)
  waiting for transfers between devices  24.7 us (10%)
  other arithmetic  18.4 us (7%)
  between operations  13.5 us (5%)
  local copies, waits for them, and re-layouts  2.64 us (1%)
    psum x1, blocking collectives, per_device(): lax.psum((lax.dynamic_update_slice(blank_rows, shift_part, corner), lax.d...  42.5 us
    dot_general x21, matrix products, project(): return jnp.dot(rows, weight, preferred_element_type=jnp.float32)  33.4 us
    all_gather x1, blocking collectives, per_device(): lax.all_gather(ctx_codes, 'sp', axis=0, tiled=True)  31.5 us
    all_gather x1, blocking collectives, per_device(): lax.all_gather(key_rot, 'sp', axis=0, tiled=True)  31.2 us
    all_gather x1, blocking collectives, per_device(): lax.all_gather(ctx_rot, 'sp', axis=0, tiled=True)  26.1 us
    reduce_scatter x1, waiting for transfers between devices, per_device(): lax.psum_scatter(project(gated, out_w).astype(jnp.bfloat16), 'tp', scatte...  24.7 us
    dot_general x5, matrix products, attend(): jnp.einsum('qhd,kd->hqk', q_rot, rotary, preferred_element_type=jnp.float32)  10.2 us
    dot_general x5, matrix products, attend(): jnp.einsum('hqk,khd->hqd', weights.astype(jnp.bfloat16), value_block.resh...  8.97 us
  transfers between devices with their start and end apart: 3, of which 1 were waited for; matrix products, arithmetic and copies ran while one was open for 7% of the time, Pallas kernels for 0%

commit v1 on v0

--- a/solution.py
+++ b/solution.py
@@ -151,7 +151,9 @@
     )
     ctx_all_codes, ctx_all_rot = (
         lax.all_gather(ctx_codes, "sp", axis=0, tiled=True),
-        lax.all_gather(ctx_rot, "sp", axis=0, tiled=True),
+        jnp.concatenate(
+            lax.all_to_all(jnp.stack([ctx_rot] * lax.axis_size("sp")), "sp", 0, 0), axis=0
+        ),
     )
     ctx_keys, ctx_values = expand(ctx_all_codes)
     running = attend(start_state, ctx_keys, ctx_values, ctx_all_rot)

time: 251 us -> 233 us (0.928)
  blocking collectives: 131 us -> 106 us
  starting transfers between devices: 0.09 us -> 5.44 us
    all_gather x1 -> x0, blocking collectives: 26.1 us -> none  [per_device(): lax.all_gather(ctx_rot, 'sp', axis=0, tiled=True)]
    all_to_all x0 -> x1, starting transfers between devices: none -> 5.32 us  [per_device(): lax.all_to_all(jnp.stack([ctx_rot] * lax.axis_size('sp')), 'sp', 0, 0)]
  transfers between devices with their start and end apart: 3 -> 4, of which waited for: 1 -> 2; matrix products, arithmetic and copies ran while one was open for 7% -> 7% of each run, Pallas kernels for 0% -> 0%
where the time goes in v1:
time: 233 us; the launch traced here: 232 us
  blocking collectives  106 us (45%)
  matrix products  58.5 us (25%)
  waiting for transfers between devices  26.3 us (11%)
  other arithmetic  18.4 us (8%)
  between operations  13.5 us (6%)
  starting transfers between devices  5.44 us (2%)
  local copies, waits for them, and re-layouts  3.35 us (1%)
    psum x1, blocking collectives, per_device(): lax.psum((lax.dynamic_update_slice(blank_rows, shift_part, corner), lax.d...  42.4 us
    dot_general x21, matrix products, project(): return jnp.dot(rows, weight, preferred_element_type=jnp.float32)  33.4 us
    all_gather x1, blocking collectives, per_device(): lax.all_gather(ctx_codes, 'sp', axis=0, tiled=True)  32 us
    all_gather x1, blocking collectives, per_device(): lax.all_gather(key_rot, 'sp', axis=0, tiled=True)  31.4 us
    reduce_scatter x1, waiting for transfers between devices, per_device(): lax.psum_scatter(project(gated, out_w).astype(jnp.bfloat16), 'tp', scatte...  25.8 us
    dot_general x5, matrix products, attend(): jnp.einsum('qhd,kd->hqk', q_rot, rotary, preferred_element_type=jnp.float32)  10.2 us
    dot_general x5, matrix products, attend(): jnp.einsum('hqk,khd->hqd', weights.astype(jnp.bfloat16), value_block.resh...  8.97 us
    reduce_sum x5, other arithmetic, attend(): row_total = row_total * factor + jnp.sum(weights, axis=-1)  8.21 us
  transfers between devices with their start and end apart: 4, of which 2 were waited for; matrix products, arithmetic and copies ran while one was open for 7% of the time, Pallas kernels for 0%

profile of v1, /device:TPU:0, one launch (start us, length us, event | category | flops | bytes accessed | tf_op | source)
XLA Modules:
  0.0 231.7 jit_solution(16089523521966412484)
XLA Ops:
  11.7 42.4 %all-reduce = (f32[2,2048]{1,0:T(2,128)S(1)}, f32[2,2048]{1,0:T(2,128)S(1)}, f32[2,2048]{1,0:T(2,128)S(1)}) all-reduce(f32[2,2048]{1,0:T(2,128)S(1)} %convolution_dynamic-update-slice_fusion, f32[2,2048]{1,0:T(2,128)S(1)} %convolution_dynamic-update-slice_fusion.1, ...), channel_id=1, replica_groups=mesh['sp'=8,'tp'=4] {'sp','tp'}, use_global_device_ids=true, to_apply=%region_2.3 | all-reduce | flops 12288 | bytes 98304 | tf_op jit(solution)/shard_map/psum | solution.py:76
  56.1 5.3 %all-to-all-start = ((bf16[8,128,32]{1,2,0:T(8,128)(2,1)}), bf16[8,128,32]{1,2,0:T(8,128)(2,1)S(1)}, u32[]{:S(2)}, u32[]{:S(2)}) async-start(bf16[8,128,32]{1,2,0:T(8,128)(2,1)} %stack.40), calls=%async_computation | async-start | bytes 131072 | tf_op jit(solution)/shard_map/all_to_all | solution.py:155
  61.5 1.8 fusion.30
  63.4 1.6 multiply_reduce_fusion.3
  65.2 32.0 %all_gather.13 = bf16[1024,256]{1,0:T(8,128)(2,1)S(1)} all-gather(bf16[128,256]{1,0:T(8,128)(2,1)S(1)} %multiply_convert_fusion.3), channel_id=1, replica_groups=mesh['sp'=8,'tp'=4] {'sp'}, dimensions={0}, use_global_device_ids=true | all-gather | bytes 589824 | tf_op jit(solution)/shard_map/all_gather | solution.py:153
  100.5 3.0 %multiply_reduce_fusion.1 = (f32[320]{0:T(512)S(1)}, f32[320,512]{1,0:T(8,128)S(1)}) fusion(bf16[320,2048]{1,0:T(8,128)(2,1)} %all-gather.4.cloned.1.call-done, bf16[2048,512]{1,0:T(8,128)(2,1)} %param.29), kind=kOutput, calls=%fused_computation.49 | convolution fusion | flops 671416000 | bytes 4064512 | tf_op jit(solution)/shard_map/dot_general | solution.py:38
  104.5 2.2 multiply_reduce_fusion.2
  107.6 1.8 fusion.57
  109.6 31.4 %all-gather = bf16[8,320,32]{1,2,0:T(8,128)(2,1)S(1)} all-gather(bf16[1,320,32]{1,2,0:T(8,128)(2,1)S(1)} %bitcast.115), channel_id=1, replica_groups=mesh['sp'=8,'tp'=4] {'sp'}, dimensions={0}, use_global_device_ids=true | all-gather | bytes 184320 | tf_op jit(solution)/shard_map/all_gather | solution.py:162
  143.6 1.7 fusion.54
  145.3 2.1 fusion.20
  147.5 2.2 fusion.24
  150.2 37.6 %while.14 = (s32[]{:T(128)}, f32[8,320]{1,0:T(8,128)S(1)}, f32[8,320]{1,0:T(8,128)S(1)}, f32[8,320,64]{1,2,0:T(8,128)S(1)}, bf16[4,640,256]{2,1,0:T(8,128)(2,1)}...) while((s32[]{:T(128)}, f32[8,320]{1,0:T(8,128)S(1)}, ...), condition=%wide.region_11.12_spmd, body=%wide.region_8.11_spmd.sunk | while | flops 872289280 | bytes 39624860 | solution.py:185
  152.7 2.2 fusion.112
  157.8 1.7 fusion.114
  162.1 2.2 fusion.112
  167.2 1.7 fusion.114
  171.5 2.2 fusion.112
  176.6 1.7 fusion.114
  180.9 2.2 fusion.112
  186.0 1.7 fusion.114
  190.1 4.8 %convolution_convert_fusion.2 = bf16[320,2048]{1,0:T(8,128)(2,1)} fusion(bf16[512,2048]{1,0:T(8,128)(2,1)S(1)} %copy-done, f32[320,512]{1,0:T(8,128)S(1)} %copy.41, bf16[320,2048]{1,0:T(8,128)(2,1)} %all-gather.4.cloned.1.call-done, bf16[2048,512]{1,0:T(8,128)(2,1)} %param.32), kind=kOutput, calls=%fused_computation.28 | convolution fusion | flops 1344143360 | bytes 7471104 | tf_op jit(solution)/shard_map/dot_general | solution.py:38
  194.9 25.8 %reduce-scatter.2.cloned.1.call-done = bf16[80,2048]{1,0:T(8,128)(2,1)} async-done(((bf16[320,2048]{1,0:T(8,128)(2,1)}), bf16[80,2048]{1,0:T(8,128)(2,1)}) %reduce-scatter.2.cloned.1.call-update) | async-done | bytes 327696 | tf_op jit(solution)/shard_map/reduce_scatter | solution.py:192
  223.2 1.9 add_convert_fusion.1
  (119 shorter events, 42.2 us)
Async XLA Ops:
  6.5 183.6 %copy-start = (bf16[512,2048]{1,0:T(8,128)(2,1)S(1)}, bf16[512,2048]{1,0:T(8,128)(2,1)}, u32[]{:S(2)}) copy-start(bf16[512,2048]{1,0:T(8,128)(2,1)} %param.39) | copy-start | bytes 6291460
  6.5 56.9 %copy-start.14 = (bf16[128,2048]{1,0:T(8,128)(2,1)S(1)}, bf16[128,2048]{1,0:T(8,128)(2,1)}, u32[]{:S(2)}) copy-start(bf16[128,2048]{1,0:T(8,128)(2,1)} %param.23) | copy-start | bytes 1572868
  6.5 58.5 %copy-start.13 = (f32[256]{0:T(256)S(1)}, f32[256]{0:T(256)}, u32[]{:S(2)}) copy-start(f32[256]{0:T(256)} %param.34) | copy-start | bytes 3076
  10.5 86.7 %copy-start.1 = (bf16[256,512]{1,0:T(8,128)(2,1)S(1)}, bf16[256,512]{1,0:T(8,128)(2,1)}, u32[]{:S(2)}) copy-start(bf16[256,512]{1,0:T(8,128)(2,1)} %param.37) | copy-start | bytes 786436
  56.1 44.2 %all-to-all-start = ((bf16[8,128,32]{1,2,0:T(8,128)(2,1)}), bf16[8,128,32]{1,2,0:T(8,128)(2,1)S(1)}, u32[]{:S(2)}, u32[]{:S(2)}) async-start(bf16[8,128,32]{1,2,0:T(8,128)(2,1)} %stack.40), calls=%async_computation | async-start | bytes 131072 | tf_op jit(solution)/shard_map/all_to_all | solution.py:155
  61.4 39.0 %all-gather.4.cloned.1.call-start = ((), (), s32[]{:S(2)}) async-start(), calls=%async_computation.2 | async-start | bytes 1638400 | tf_op jit(solution)/shard_map/all_gather | solution.py:91
  61.5 37.2 %copy-start.2 = (bf16[256,512]{1,0:T(8,128)(2,1)S(1)}, bf16[256,512]{1,0:T(8,128)(2,1)}, u32[]{:S(2)}) copy-start(bf16[256,512]{1,0:T(8,128)(2,1)} %param.38) | copy-start | bytes 786436
  63.3 86.8 %all-gather.6.cloned.1.call-start = ((), (), s32[]{:S(2)}) async-start(), calls=%async_computation.3 | async-start | bytes 1474560 | tf_op jit(solution)/shard_map/all_gather | solution.py:161
  100.4 3.1 %copy-start.8 = (bf16[512,256]{1,0:T(8,128)(2,1)S(1)}, bf16[512,256]{1,0:T(8,128)(2,1)}, u32[]{:S(2)}) copy-start(bf16[512,256]{1,0:T(8,128)(2,1)} %param.36) | copy-start | bytes 786436
  100.4 3.1 %copy-start.12 = (f32[512]{0:T(512)S(1)}, f32[512]{0:T(512)}, u32[]{:S(2)}) copy-start(f32[512]{0:T(512)} %param.33) | copy-start | bytes 6148
  100.5 3.4 %copy-start.7 = (bf16[512,512]{1,0:T(8,128)(2,1)S(1)}, bf16[512,512]{1,0:T(8,128)(2,1)}, u32[]{:S(2)}) copy-start(bf16[512,512]{1,0:T(8,128)(2,1)} %param.35) | copy-start | bytes 1572868
  104.3 3.3 %copy-start.9 = (bf16[2048,32]{0,1:T(8,128)(2,1)S(1)}, bf16[2048,32]{0,1:T(8,128)(2,1)}, u32[]{:S(2)}) copy-start(bf16[2048,32]{0,1:T(8,128)(2,1)} %param.31) | copy-start | bytes 393220
  107.6 113.2 %reduce-scatter.2.cloned.1.call-start = ((), (), s32[]{:S(2)}) async-start(), calls=%async_computation.4 | async-start | bytes 1638400 | tf_op jit(solution)/shard_map/reduce_scatter | solution.py:192
  142.0 1.6 copy-start.5
  145.3 2.2 copy-start.6
  154.9 1.6 copy-start.3
  164.3 1.6 copy-start.3
  173.7 1.6 copy-start.3
  183.1 1.6 copy-start.3
  190.1 30.6 %copy-start.4 = (bf16[80,2048]{1,0:T(8,128)(2,1)S(1)}, bf16[80,2048]{1,0:T(8,128)(2,1)}, u32[]{:S(2)}) copy-start(bf16[80,2048]{1,0:T(8,128)(2,1)} %param.22) | copy-start | bytes 983044
  194.9 28.3 %copy-start.10 = (f32[2048]{0:T(1024)S(1)}, f32[2048]{0:T(1024)}, u32[]{:S(2)}) copy-start(f32[2048]{0:T(1024)} %param.41) | copy-start | bytes 24580
  194.9 28.3 %copy-start.11 = (f32[2048]{0:T(1024)S(1)}, f32[2048]{0:T(1024)}, u32[]{:S(2)}) copy-start(f32[2048]{0:T(1024)} %param.40) | copy-start | bytes 24580
Sparse Core Ops, SparseCore 0:
  63.8 18.6 all-gather.3
  107.7 42.4 all-gather.5
  195.0 25.6 reduce-scatter.1
